TPU v7x, 512 devices: a whole 4x4x16 slice. The times are simulated.
512 devices in a mesh: gr: 2 (over z_hi), fs: 32 (over z_lo, y), tp: 8 (over x, core).
Axes of the slice: x: 4, y: 4, z: 16 (z_hi: 2, z_lo: 8; z = z_hi * 8 + z_lo), core: 2. Of those that a mesh axis runs over, the one named last changes fastest.
Arguments:
- tokens: bfloat16 [24576, 2048], P(('gr', 'fs')), may hold values from -6 to 6
- route_ids: int32 [24576, 2], P(('gr', 'fs')), may hold values from 0 to 31, as said below
- route_weights: float32 [24576, 2], P(('gr', 'fs')), may hold values from 0.1 to 1
- norm_gain: float32 [2048], P(('gr', 'fs')), may hold values from 0.1 to 1.9
- gate_weight: float32 [32, 2048, 1024], P(None, ('gr', 'fs'), 'tp'), may hold values from -0.125 to 0.125
- up_weight: float32 [32, 2048, 1024], P(None, ('gr', 'fs'), 'tp'), may hold values from -0.125 to 0.125
- down_weight: float32 [32, 1024, 2048], P(None, ('gr', 'fs'), 'tp'), may hold values from -0.1875 to 0.1875
Outputs:
- gate_new: bfloat16 [32, 2048, 1024], P('fs', None, 'tp')
- up_new: bfloat16 [32, 2048, 1024], P('fs', None, 'tp')
- down_new: bfloat16 [32, 1024, 2048], P('fs', 'tp')
- mixed: bfloat16 [24576, 2048], P(('gr', 'fs'), 'tp')
Inputs may be any that keep to these rules, and one draw needn't show every extreme that they name: `route_ids`: each row names two different experts of one group (expert e belongs to group e // 8); in each device's block of 384 rows every expert is named by exactly 24 rows.
All inputs are finite; a program needn't handle non-finite values.
Results may differ from a plain program's by a relative error of at most 0.015.
Values may be sent and summed in bfloat16 or wider, within the bound.
A program may use at most 64 MiB of HBM per device.

v0:
```python
import jax
import jax.numpy as jnp
from jax import lax
from jax.sharding import Mesh
from jax.sharding import PartitionSpec as P

TP = ("tp_0", "tp_1")


def side_by_side(arrays, axis, split_dim, concat_dim, along):
    ends, at = ([], 0)
    for a in arrays[:-1]:
        at += a.shape[along]
        ends.append(at)
    both = jnp.concatenate(arrays, axis=along)
    return tuple(
        jnp.split(
            lax.all_to_all(both, axis, split_axis=split_dim, concat_axis=concat_dim, tiled=True),
            ends,
            axis=along,
        )
    )


def in_one_piece(arrays, axis, dim, along):
    ends, at = ([], 0)
    for a in arrays[:-1]:
        at += a.shape[along]
        ends.append(at)
    both = jnp.concatenate(arrays, axis=along)
    return tuple(jnp.split(lax.all_gather(both, axis, axis=dim, tiled=True), ends, axis=along))


def split_up(array, dim, devices):
    before, after = (array.shape[:dim], array.shape[dim + 1 :])
    return jnp.moveaxis(array.reshape(*before, devices, -1, *after), dim, 0)


def laid_out(pieces, dim):
    pieces = jnp.moveaxis(pieces, 0, dim)
    lengths = pieces.shape
    return pieces.reshape(*lengths[:dim], lengths[dim] * lengths[dim + 1], *lengths[dim + 2 :])


def exchange_in_order(pieces, axes, turns):
    inside = pieces.shape[1:]
    whole = pieces.reshape(*(lax.axis_size(a) for a in axes), *inside)
    for k in turns:
        whole = lax.all_to_all(whole, axes[k], k, k, tiled=True)
    return whole.reshape(-1, *inside)


def exchange_by_axis(array, axes, turns, split_dim, concat_dim):
    pieces = split_up(array, split_dim, lax.axis_size(axes))
    return laid_out(exchange_in_order(pieces, axes, turns), concat_dim)


def local(tokens, route_ids, route_weights, norm_gain, gate_weight, up_weight, down_weight):
    gate_folded = (gate_weight * norm_gain[None, :, None]).astype(jnp.bfloat16)
    up_folded = (up_weight * norm_gain[None, :, None]).astype(jnp.bfloat16)
    down_rounded = down_weight.astype(jnp.bfloat16)
    moved = (
        *side_by_side((gate_folded, up_folded), "fs", 0, 1, 2),
        lax.all_to_all(down_rounded, "fs", split_axis=0, concat_axis=1, tiled=True),
    )
    gate_new, up_new, down_whole = (
        *in_one_piece((moved[0], moved[1]), "gr", 1, 0),
        lax.all_gather(moved[2], "gr", axis=1, tiled=True),
    )
    down_new = exchange_by_axis(down_whole, TP, (1, 0), 1, 2)
    tok = tokens.shape[0]
    width = tokens.shape[1]
    experts = gate_weight.shape[0]
    cap = 2 * tok // experts
    flat_ids = route_ids.reshape(-1)
    onehot = (flat_ids[:, None] == jnp.arange(experts, dtype=jnp.int32)[None, :]).astype(jnp.int32)
    slot = jnp.sum(jnp.cumsum(onehot, axis=0) * onehot, axis=1) - 1
    position = flat_ids * cap + slot
    source = (
        jnp.zeros((experts * cap,), jnp.int32)
        .at[position]
        .set(jnp.arange(2 * tok, dtype=jnp.int32) // 2)
    )
    widened = tokens.astype(jnp.float32)
    normed = (
        widened * lax.rsqrt(jnp.mean(widened * widened, axis=-1, keepdims=True) + 1e-06)
    ).astype(jnp.bfloat16)
    outgoing = normed[source].reshape(experts, cap, width)
    received = lax.all_to_all(outgoing, "fs", split_axis=0, concat_axis=0, tiled=True)
    senders, count, _ = received.shape
    rows = received.reshape(senders * count, width)
    first = jnp.dot(rows, gate_new[0], preferred_element_type=jnp.float32)
    second = jnp.dot(rows, up_new[0], preferred_element_type=jnp.float32)
    hidden = (jax.nn.silu(first) * second).astype(jnp.bfloat16)
    hidden_width = hidden.shape[1]
    down_local = down_whole[0]
    out_columns = down_local.shape[1]
    row_count = hidden.shape[0]
    piece = lax.all_gather(hidden, TP, axis=1, tiled=True)
    piece_width = piece.shape[1]
    blocks = piece_width // hidden_width
    partials = jnp.einsum(
        "mbf,bfd->bmd",
        piece.reshape(row_count, blocks, hidden_width),
        down_local.reshape(blocks, hidden_width, out_columns),
        preferred_element_type=jnp.float32,
    ).astype(jnp.bfloat16)
    total = jnp.sum(partials.astype(jnp.float32), axis=0)
    summed = total.reshape(senders, count, out_columns)
    returned = lax.all_to_all(
        summed.astype(jnp.bfloat16), "fs", split_axis=0, concat_axis=0, tiled=True
    )
    columns = returned.shape[2]
    route_out = returned.reshape(experts * cap, columns)[position].reshape(tok, 2, columns)
    mixed = jnp.sum(route_weights[:, :, None] * route_out.astype(jnp.float32), axis=1).astype(
        jnp.bfloat16
    )
    return (gate_new, up_new, down_new, mixed)


def solution(mesh):
    torus = Mesh(
        mesh.devices.reshape(mesh.shape["gr"], mesh.shape["fs"], 4, 2), ("gr", "fs", "tp_0", "tp_1")
    )
    placed = (
        P(("gr", "fs"), None),
        P(("gr", "fs"), None),
        P(("gr", "fs"), None),
        P(("gr", "fs")),
        P(None, ("gr", "fs"), TP),
        P(None, ("gr", "fs"), TP),
        P(None, ("gr", "fs"), TP),
    )
    return jax.shard_map(
        local,
        mesh=torus,
        in_specs=placed,
        out_specs=(P("fs", None, TP), P("fs", None, TP), P("fs", TP, None), P(("gr", "fs"), TP)),
        check_vma=False,
    )
```

profile of v0, /device:TPU:2, one launch (start us, length us, event | category | flops | bytes accessed | tf_op | source)
XLA Modules:
  0.0 370.6 jit_solution(3223288350482646378)
XLA Ops:
  7.2 0.0 copy-start.2
  7.2 0.0 copy-start
  7.2 1.5 multiply_convert_fusion.1
  8.7 0.9 pad_maximum_fusion
  9.6 15.7 %all-to-all-start = ((bf16[32,32,256]{2,1,0:T(8,128)(2,1)}), bf16[32,32,256]{2,1,0:T(8,128)(2,1)}, u32[]{:S(2)}, u32[]{:S(2)}) async-start(bf16[32,32,256]{2,1,0:T(8,128)(2,1)} %pad_maximum_fusion), calls=%async_computation | async-start | bytes 1048576 | tf_op jit(solution)/shard_map/all_to_all | solution.py:18
  25.2 0.0 copy-done.2
  25.2 0.1 copy.34
  25.4 0.1 eq.29
  25.5 0.1 eq.25
  25.7 1.7 reduce-window.6
  27.4 0.3 slice_reduce_fusion
  27.7 0.1 copy.33
  27.9 0.2 mul.68
  28.1 0.1 fusion.9
  28.2 3.4 scatter_custom_fusion
  31.6 0.0 copy-done
  31.6 0.4 fusion
  32.0 0.3 fusion.1
  32.4 4.3 %gather_fusion = bf16[768,2048]{1,0:T(8,128)(2,1)} fusion(bf16[384,2048]{1,0:T(8,128)(2,1)S(1)} %fusion.1, s32[1024]{0:T(1024)S(1)} %pad_clamp_fusion.1), kind=kCustom, calls=%fused_computation | custom fusion | bytes 6294528 | tf_op jit(solution)/shard_map/gather | solution.py:88
  36.6 18.2 %all-to-all-done = bf16[32,32,256]{2,1,0:T(8,128)(2,1)} async-done(((bf16[32,32,256]{2,1,0:T(8,128)(2,1)}), bf16[32,32,256]{2,1,0:T(8,128)(2,1)}, u32[]{:S(2)}, u32[]{:S(2)}) %all-to-all-start) | async-done | bytes 524320 | tf_op jit(solution)/shard_map/all_to_all | solution.py:18
  54.8 6.1 %all-to-all-start.4 = ((bf16[32,24,2048]{2,1,0:T(8,128)(2,1)}), bf16[32,24,2048]{2,1,0:T(8,128)(2,1)S(1)}, u32[]{:S(2)}, u32[]{:S(2)}) async-start(bf16[32,24,2048]{2,1,0:T(8,128)(2,1)} %bitcast.48), calls=%async_computation.4 | async-start | bytes 6291456 | tf_op jit(solution)/shard_map/all_to_all | solution.py:89
  60.9 0.0 all-gather.3.cloned.1.call-start
  61.0 1.1 fusion.18
  62.1 0.8 pad_maximum_fusion.1
  62.9 0.0 all-gather.3.cloned.1.call-update
  62.9 0.0 all-gather.5.cloned.1.call-start
  63.0 66.8 %all-gather.3.cloned.1.call-done = bf16[2,2048,128]{2,1,0:T(8,128)(2,1)} async-done(((bf16[2,1024,128]{2,1,0:T(8,128)(2,1)}), bf16[2,2048,128]{2,1,0:T(8,128)(2,1)}) %all-gather.3.cloned.1.call-update) | async-done | bytes 1048592 | tf_op jit(solution)/shard_map/all_gather | solution.py:31
  129.8 2.2 fusion.17
  132.0 114.4 %all-to-all-done.4 = bf16[32,24,2048]{2,1,0:T(8,128)(2,1)S(1)} async-done(((bf16[32,24,2048]{2,1,0:T(8,128)(2,1)}), bf16[32,24,2048]{2,1,0:T(8,128)(2,1)S(1)}, u32[]{:S(2)}, u32[]{:S(2)}) %all-to-all-start.4) | async-done | bytes 3145760 | tf_op jit(solution)/shard_map/all_to_all | solution.py:89
  246.4 2.1 fusion.6
  248.5 0.0 copy-done.1
  248.5 1.7 fusion.4
  250.2 0.0 all-gather.5.cloned.1.call-update
  250.2 1.1 convert_element_type.42
  251.3 26.3 %all_to_all.44 = bf16[32,16,256]{2,1,0:T(8,128)(2,1)S(1)} all-to-all(bf16[32,16,256]{2,1,0:T(8,128)(2,1)S(1)} %convert_element_type.42), channel_id=1, replica_groups=mesh['gr'=2,'fs'=32,'tp_0'=4,'tp_1'=2] {'fs'}, dimensions={0} | all-to-all | bytes 524288 | tf_op jit(solution)/shard_map/all_to_all | solution.py:64
  277.6 29.7 %all_gather.10 = bf16[1,1024,256]{2,1,0:T(8,128)(2,1)S(1)} all-gather(bf16[1,512,256]{2,1,0:T(8,128)(2,1)S(1)} %bitcast.52), channel_id=1, replica_groups=mesh['gr'=2,'fs'=32,'tp_0'=4,'tp_1'=2] {'gr'}, dimensions={1}, use_global_device_ids=true | all-gather | bytes 786432 | tf_op jit(solution)/shard_map/all_gather | solution.py:68
  307.3 4.2 %all_to_all.45 = bf16[4,2,1,128,256]{4,3,0,2,1:T(8,128)(2,1)S(1)} all-to-all(bf16[4,2,1,128,256]{4,3,0,2,1:T(8,128)(2,1)S(1)} %copy.29), channel_id=1, replica_groups=mesh['gr'=2,'fs'=32,'tp_0'=4,'tp_1'=2] {'tp_1'}, dimensions={1} | all-to-all | bytes 1048576 | tf_op jit(solution)/shard_map/all_to_all | solution.py:49
  311.5 0.8 copy.30
  312.3 5.0 %all-to-all-start.3 = ((bf16[4,2,1,128,256]{4,3,1,2,0:T(8,128)(2,1)}), bf16[4,2,1,128,256]{4,3,1,2,0:T(8,128)(2,1)S(1)}, u32[]{:S(2)}, u32[]{:S(2)}) async-start(bf16[4,2,1,128,256]{4,3,1,2,0:T(8,128)(2,1)} %copy.30), calls=%async_computation.3 | async-start | bytes 1048576 | tf_op jit(solution)/shard_map/all_to_all | solution.py:49
  317.3 3.2 convert_reduce_fusion
  320.5 5.1 %all-to-all-done.3 = bf16[4,2,1,128,256]{4,3,1,2,0:T(8,128)(2,1)S(1)} async-done(((bf16[4,2,1,128,256]{4,3,1,2,0:T(8,128)(2,1)}), bf16[4,2,1,128,256]{4,3,1,2,0:T(8,128)(2,1)S(1)}, u32[]{:S(2)}, u32[]{:S(2)}) %all-to-all-start.3) | async-done | bytes 524320 | tf_op jit(solution)/shard_map/all_to_all | solution.py:49
  325.6 10.0 %all-to-all-start.5 = ((bf16[32,24,256]{2,1,0:T(8,128)(2,1)}), bf16[32,24,256]{2,1,0:T(8,128)(2,1)S(1)}, u32[]{:S(2)}, u32[]{:S(2)}) async-start(bf16[32,24,256]{2,1,0:T(8,128)(2,1)} %bitcast.11), calls=%async_computation.5 | async-start | bytes 786432 | tf_op jit(solution)/shard_map/all_to_all | solution.py:110
  335.6 0.1 copy.32
  335.7 0.8 copy.39
  336.6 22.4 %all-to-all-done.5 = bf16[32,24,256]{2,1,0:T(8,128)(2,1)S(1)} async-done(((bf16[32,24,256]{2,1,0:T(8,128)(2,1)}), bf16[32,24,256]{2,1,0:T(8,128)(2,1)S(1)}, u32[]{:S(2)}, u32[]{:S(2)}) %all-to-all-start.5) | async-done | bytes 393248 | tf_op jit(solution)/shard_map/all_to_all | solution.py:110
  359.0 2.6 gather_fusion.1
  361.6 0.4 reshape.105
  362.0 1.7 multiply_reduce_fusion
  (15 shorter events, 0.1 us)
Async XLA Ops:
  7.2 18.1 %copy-start.2 = (s32[384,2]{0,1:T(2,128)S(1)}, s32[384,2]{0,1:T(2,128)}, u32[]{:S(2)}) copy-start(s32[384,2]{0,1:T(2,128)} %param.8) | copy-start | bytes 9220
  7.2 24.4 %copy-start = (bf16[384,2048]{1,0:T(8,128)(2,1)S(1)}, bf16[384,2048]{1,0:T(8,128)(2,1)}, u32[]{:S(2)}) copy-start(bf16[384,2048]{1,0:T(8,128)(2,1)} %param.7) | copy-start | bytes 4718596
  9.6 45.3 %all-to-all-start = ((bf16[32,32,256]{2,1,0:T(8,128)(2,1)}), bf16[32,32,256]{2,1,0:T(8,128)(2,1)}, u32[]{:S(2)}, u32[]{:S(2)}) async-start(bf16[32,32,256]{2,1,0:T(8,128)(2,1)} %pad_maximum_fusion), calls=%async_computation | async-start | bytes 1048576 | tf_op jit(solution)/shard_map/all_to_all | solution.py:18
  54.8 191.6 %all-to-all-start.4 = ((bf16[32,24,2048]{2,1,0:T(8,128)(2,1)}), bf16[32,24,2048]{2,1,0:T(8,128)(2,1)S(1)}, u32[]{:S(2)}, u32[]{:S(2)}) async-start(bf16[32,24,2048]{2,1,0:T(8,128)(2,1)} %bitcast.48), calls=%async_computation.4 | async-start | bytes 6291456 | tf_op jit(solution)/shard_map/all_to_all | solution.py:89
  60.9 68.8 %all-gather.3.cloned.1.call-start = ((), (), s32[]{:S(2)}) async-start(), calls=%async_computation.6 | async-start | bytes 1572864 | tf_op jit(solution)/shard_map/all_gather | solution.py:31
  62.9 254.4 %all-gather.5.cloned.1.call-start = ((), (), s32[]{:S(2)}) async-start(), calls=%async_computation.7 | async-start | bytes 1769472 | tf_op jit(solution)/shard_map/all_gather | solution.py:99
  246.4 2.1 copy-start.1
  312.3 23.3 %copy-start.3 = (f32[384,2]{0,1:T(2,128)S(1)}, f32[384,2]{0,1:T(2,128)}, u32[]{:S(2)}) copy-start(f32[384,2]{0,1:T(2,128)} %param.9) | copy-start | bytes 9220
  312.3 13.3 %all-to-all-start.3 = ((bf16[4,2,1,128,256]{4,3,1,2,0:T(8,128)(2,1)}), bf16[4,2,1,128,256]{4,3,1,2,0:T(8,128)(2,1)S(1)}, u32[]{:S(2)}, u32[]{:S(2)}) async-start(bf16[4,2,1,128,256]{4,3,1,2,0:T(8,128)(2,1)} %copy.30), calls=%async_computation.3 | async-start | bytes 1048576 | tf_op jit(solution)/shard_map/all_to_all | solution.py:49
  325.6 33.4 %all-to-all-start.5 = ((bf16[32,24,256]{2,1,0:T(8,128)(2,1)}), bf16[32,24,256]{2,1,0:T(8,128)(2,1)S(1)}, u32[]{:S(2)}, u32[]{:S(2)}) async-start(bf16[32,24,256]{2,1,0:T(8,128)(2,1)} %bitcast.11), calls=%async_computation.5 | async-start | bytes 786432 | tf_op jit(solution)/shard_map/all_to_all | solution.py:110
Sparse Core Ops, SparseCore 0:
  64.4 65.2 all-gather.2
  250.3 28.7 all-gather.4
where the time goes:
time: 371 us
  waiting for transfers between devices  227 us (61%)
  blocking collectives  60.1 us (16%)
  starting transfers between devices  36.8 us (10%)
  local copies, waits for them, and re-layouts  16.8 us (5%)
  between operations  14.3 us (4%)
  other arithmetic  8.64 us (2%)
  matrix products  6.94 us (2%)
    all_to_all x1, waiting for transfers between devices, local(): lax.all_to_all(outgoing, 'fs', split_axis=0, concat_axis=0, tiled=True)  114 us
    all_gather x1, waiting for transfers between devices, in_one_piece(): lax.all_gather(both, axis, axis=dim, tiled=True)  66.8 us
    all_gather x1, blocking collectives, local(): lax.all_gather(moved[2], 'gr', axis=1, tiled=True)  29.7 us
    all_to_all x1, blocking collectives, local(): lax.all_to_all(down_rounded, 'fs', split_axis=0, concat_axis=1, tiled=True)  26.3 us
    all_to_all x1, waiting for transfers between devices, local(): lax.all_to_all(summed.astype(jnp.bfloat16), 'fs', split_axis=0, concat_ax...  22.4 us
    all_to_all x1, waiting for transfers between devices, side_by_side(): lax.all_to_all(both, axis, split_axis=split_dim, concat_axis=concat_dim,...  18.2 us
    all_to_all x1, starting transfers between devices, side_by_side(): lax.all_to_all(both, axis, split_axis=split_dim, concat_axis=concat_dim,...  15.7 us
    all_to_all x1, starting transfers between devices, local(): lax.all_to_all(summed.astype(jnp.bfloat16), 'fs', split_axis=0, concat_ax...  9.96 us
  transfers between devices with their start and end apart: 6, of which 5 were waited for; matrix products, arithmetic and copies ran while one was open for 6% of the time, Pallas kernels for 0%

commit v1 on v0

--- a/solution.py
+++ b/solution.py
@@ -65,7 +65,9 @@
     )
     gate_new, up_new, down_whole = (
         *in_one_piece((moved[0], moved[1]), "gr", 1, 0),
-        lax.all_gather(moved[2], "gr", axis=1, tiled=True),
+        jnp.concatenate(
+            lax.all_to_all(jnp.stack([moved[2]] * lax.axis_size("gr")), "gr", 0, 0), axis=1
+        ),
     )
     down_new = exchange_by_axis(down_whole, TP, (1, 0), 1, 2)
     tok = tokens.shape[0]

time: 371 us -> 376 us (1.013)
  blocking collectives: 60.1 us -> 65.1 us
    all_to_all x0 -> x1, blocking collectives: none -> 34.7 us  [local(): lax.all_to_all(jnp.stack([moved[2]] * lax.axis_size('gr')), 'gr', 0, 0)]
    all_gather x1 -> x0, blocking collectives: 29.7 us -> none  [local(): lax.all_gather(moved[2], 'gr', axis=1, tiled=True)]
where the time goes in v1:
time: 376 us; the launch traced here: 375 us
  waiting for transfers between devices  227 us (60%)
  blocking collectives  65.1 us (17%)
  starting transfers between devices  36.2 us (10%)
  local copies, waits for them, and re-layouts  16.8 us (4%)
  between operations  14.3 us (4%)
  other arithmetic  8.68 us (2%)
  matrix products  6.93 us (2%)
    all_to_all x1, waiting for transfers between devices, local(): lax.all_to_all(outgoing, 'fs', split_axis=0, concat_axis=0, tiled=True)  114 us
    all_gather x1, waiting for transfers between devices, in_one_piece(): lax.all_gather(both, axis, axis=dim, tiled=True)  66.8 us
    all_to_all x1, blocking collectives, local(): lax.all_to_all(jnp.stack([moved[2]] * lax.axis_size('gr')), 'gr', 0, 0)  34.7 us
    all_to_all x1, blocking collectives, local(): lax.all_to_all(down_rounded, 'fs', split_axis=0, concat_axis=1, tiled=True)  26.3 us
    all_to_all x1, waiting for transfers between devices, local(): lax.all_to_all(summed.astype(jnp.bfloat16), 'fs', split_axis=0, concat_ax...  22.4 us
    all_to_all x1, waiting for transfers between devices, side_by_side(): lax.all_to_all(both, axis, split_axis=split_dim, concat_axis=concat_dim,...  18.2 us
    all_to_all x1, starting transfers between devices, side_by_side(): lax.all_to_all(both, axis, split_axis=split_dim, concat_axis=concat_dim,...  15.7 us
    all_to_all x1, starting transfers between devices, local(): lax.all_to_all(summed.astype(jnp.bfloat16), 'fs', split_axis=0, concat_ax...  9.41 us
  transfers between devices with their start and end apart: 6, of which 5 were waited for; matrix products, arithmetic and copies ran while one was open for 6% of the time, Pallas kernels for 0%

profile of v1, /device:TPU:2, one launch (start us, length us, event | category | flops | bytes accessed | tf_op | source)
XLA Modules:
  0.0 375.1 jit_solution(13393855138463906271)
XLA Ops:
  7.2 0.0 copy-start.2
  7.2 0.0 copy-start
  7.2 1.5 multiply_convert_fusion.1
  8.7 0.9 pad_maximum_fusion
  9.6 15.7 %all-to-all-start = ((bf16[32,32,256]{2,1,0:T(8,128)(2,1)}), bf16[32,32,256]{2,1,0:T(8,128)(2,1)}, u32[]{:S(2)}, u32[]{:S(2)}) async-start(bf16[32,32,256]{2,1,0:T(8,128)(2,1)} %pad_maximum_fusion), calls=%async_computation | async-start | bytes 1048576 | tf_op jit(solution)/shard_map/all_to_all | solution.py:18
  25.2 0.0 copy-done.2
  25.2 0.1 copy.30
  25.4 0.1 eq.29
  25.5 0.1 eq.25
  25.7 1.7 reduce-window.6
  27.4 0.3 slice_reduce_fusion
  27.7 0.1 copy.29
  27.9 0.2 mul.68
  28.1 0.1 fusion.9
  28.2 3.4 scatter_custom_fusion
  31.6 0.0 copy-done
  31.6 0.4 fusion
  32.0 0.3 fusion.1
  32.4 4.3 %gather_fusion = bf16[768,2048]{1,0:T(8,128)(2,1)} fusion(bf16[384,2048]{1,0:T(8,128)(2,1)S(1)} %fusion.1, s32[1024]{0:T(1024)S(1)} %pad_clamp_fusion.1), kind=kCustom, calls=%fused_computation | custom fusion | bytes 6294528 | tf_op jit(solution)/shard_map/gather | solution.py:90
  36.6 18.2 %all-to-all-done = bf16[32,32,256]{2,1,0:T(8,128)(2,1)} async-done(((bf16[32,32,256]{2,1,0:T(8,128)(2,1)}), bf16[32,32,256]{2,1,0:T(8,128)(2,1)}, u32[]{:S(2)}, u32[]{:S(2)}) %all-to-all-start) | async-done | bytes 524320 | tf_op jit(solution)/shard_map/all_to_all | solution.py:18
  54.8 6.1 %all-to-all-start.5 = ((bf16[32,24,2048]{2,1,0:T(8,128)(2,1)}), bf16[32,24,2048]{2,1,0:T(8,128)(2,1)S(1)}, u32[]{:S(2)}, u32[]{:S(2)}) async-start(bf16[32,24,2048]{2,1,0:T(8,128)(2,1)} %bitcast.48), calls=%async_computation.5 | async-start | bytes 6291456 | tf_op jit(solution)/shard_map/all_to_all | solution.py:91
  60.9 0.0 all-gather.3.cloned.1.call-start
  61.0 1.1 fusion.18
  62.1 0.8 pad_maximum_fusion.1
  62.9 0.0 all-gather.3.cloned.1.call-update
  62.9 0.0 all-gather.5.cloned.1.call-start
  63.0 66.8 %all-gather.3.cloned.1.call-done = bf16[2,2048,128]{2,1,0:T(8,128)(2,1)} async-done(((bf16[2,1024,128]{2,1,0:T(8,128)(2,1)}), bf16[2,2048,128]{2,1,0:T(8,128)(2,1)}) %all-gather.3.cloned.1.call-update) | async-done | bytes 1048592 | tf_op jit(solution)/shard_map/all_gather | solution.py:31
  129.8 2.2 fusion.17
  132.0 114.4 %all-to-all-done.5 = bf16[32,24,2048]{2,1,0:T(8,128)(2,1)S(1)} async-done(((bf16[32,24,2048]{2,1,0:T(8,128)(2,1)}), bf16[32,24,2048]{2,1,0:T(8,128)(2,1)S(1)}, u32[]{:S(2)}, u32[]{:S(2)}) %all-to-all-start.5) | async-done | bytes 3145760 | tf_op jit(solution)/shard_map/all_to_all | solution.py:91
  246.4 2.1 fusion.6
  248.5 0.0 copy-done.1
  248.5 1.7 fusion.4
  250.2 0.0 all-gather.5.cloned.1.call-update
  250.2 1.1 convert_element_type.42
  251.3 26.3 %all_to_all.46 = bf16[32,16,256]{2,1,0:T(8,128)(2,1)S(1)} all-to-all(bf16[32,16,256]{2,1,0:T(8,128)(2,1)S(1)} %convert_element_type.42), channel_id=1, replica_groups=mesh['gr'=2,'fs'=32,'tp_0'=4,'tp_1'=2] {'fs'}, dimensions={0} | all-to-all | bytes 524288 | tf_op jit(solution)/shard_map/all_to_all | solution.py:64
  277.6 34.7 %all_to_all.47 = bf16[2,1,512,256]{3,2,1,0:T(8,128)(2,1)S(1)} all-to-all(bf16[2,1,512,256]{3,2,1,0:T(8,128)(2,1)S(1)} %pad_maximum_fusion.2), channel_id=1, replica_groups=mesh['gr'=2,'fs'=32,'tp_0'=4,'tp_1'=2] {'gr'}, dimensions={0} | all-to-all | bytes 1048576 | tf_op jit(solution)/shard_map/all_to_all | solution.py:69
  312.4 4.2 %all_to_all.48 = bf16[4,2,1,128,256]{4,3,0,2,1:T(8,128)(2,1)S(1)} all-to-all(bf16[4,2,1,128,256]{4,3,0,2,1:T(8,128)(2,1)S(1)} %copy.25), channel_id=1, replica_groups=mesh['gr'=2,'fs'=32,'tp_0'=4,'tp_1'=2] {'tp_1'}, dimensions={1} | all-to-all | bytes 1048576 | tf_op jit(solution)/shard_map/all_to_all | solution.py:49
  316.5 0.8 copy.26
  317.3 5.0 %all-to-all-start.4 = ((bf16[4,2,1,128,256]{4,3,1,2,0:T(8,128)(2,1)}), bf16[4,2,1,128,256]{4,3,1,2,0:T(8,128)(2,1)S(1)}, u32[]{:S(2)}, u32[]{:S(2)}) async-start(bf16[4,2,1,128,256]{4,3,1,2,0:T(8,128)(2,1)} %copy.26), calls=%async_computation.4 | async-start | bytes 1048576 | tf_op jit(solution)/shard_map/all_to_all | solution.py:49
  322.3 3.2 convert_reduce_fusion
  325.5 5.1 %all-to-all-done.4 = bf16[4,2,1,128,256]{4,3,1,2,0:T(8,128)(2,1)S(1)} async-done(((bf16[4,2,1,128,256]{4,3,1,2,0:T(8,128)(2,1)}), bf16[4,2,1,128,256]{4,3,1,2,0:T(8,128)(2,1)S(1)}, u32[]{:S(2)}, u32[]{:S(2)}) %all-to-all-start.4) | async-done | bytes 524320 | tf_op jit(solution)/shard_map/all_to_all | solution.py:49
  330.6 9.4 %all-to-all-start.6 = ((bf16[32,24,256]{2,1,0:T(8,128)(2,1)}), bf16[32,24,256]{2,1,0:T(8,128)(2,1)S(1)}, u32[]{:S(2)}, u32[]{:S(2)}) async-start(bf16[32,24,256]{2,1,0:T(8,128)(2,1)} %bitcast.11), calls=%async_computation.6 | async-start | bytes 786432 | tf_op jit(solution)/shard_map/all_to_all | solution.py:112
  340.0 0.1 copy.28
  340.2 0.8 copy.35
  341.1 22.4 %all-to-all-done.6 = bf16[32,24,256]{2,1,0:T(8,128)(2,1)S(1)} async-done(((bf16[32,24,256]{2,1,0:T(8,128)(2,1)}), bf16[32,24,256]{2,1,0:T(8,128)(2,1)S(1)}, u32[]{:S(2)}, u32[]{:S(2)}) %all-to-all-start.6) | async-done | bytes 393248 | tf_op jit(solution)/shard_map/all_to_all | solution.py:112
  363.5 2.6 gather_fusion.1
  366.1 0.4 reshape.106
  366.5 1.7 multiply_reduce_fusion
  (16 shorter events, 0.2 us)
Async XLA Ops:
  7.2 18.1 %copy-start.2 = (s32[384,2]{0,1:T(2,128)S(1)}, s32[384,2]{0,1:T(2,128)}, u32[]{:S(2)}) copy-start(s32[384,2]{0,1:T(2,128)} %param.8) | copy-start | bytes 9220
  7.2 24.4 %copy-start = (bf16[384,2048]{1,0:T(8,128)(2,1)S(1)}, bf16[384,2048]{1,0:T(8,128)(2,1)}, u32[]{:S(2)}) copy-start(bf16[384,2048]{1,0:T(8,128)(2,1)} %param.7) | copy-start | bytes 4718596
  9.6 45.3 %all-to-all-start = ((bf16[32,32,256]{2,1,0:T(8,128)(2,1)}), bf16[32,32,256]{2,1,0:T(8,128)(2,1)}, u32[]{:S(2)}, u32[]{:S(2)}) async-start(bf16[32,32,256]{2,1,0:T(8,128)(2,1)} %pad_maximum_fusion), calls=%async_computation | async-start | bytes 1048576 | tf_op jit(solution)/shard_map/all_to_all | solution.py:18
  54.8 191.6 %all-to-all-start.5 = ((bf16[32,24,2048]{2,1,0:T(8,128)(2,1)}), bf16[32,24,2048]{2,1,0:T(8,128)(2,1)S(1)}, u32[]{:S(2)}, u32[]{:S(2)}) async-start(bf16[32,24,2048]{2,1,0:T(8,128)(2,1)} %bitcast.48), calls=%async_computation.5 | async-start | bytes 6291456 | tf_op jit(solution)/shard_map/all_to_all | solution.py:91
  60.9 68.8 %all-gather.3.cloned.1.call-start = ((), (), s32[]{:S(2)}) async-start(), calls=%async_computation.7 | async-start | bytes 1572864 | tf_op jit(solution)/shard_map/all_gather | solution.py:31
  62.9 259.4 %all-gather.5.cloned.1.call-start = ((), (), s32[]{:S(2)}) async-start(), calls=%async_computation.8 | async-start | bytes 1769472 | tf_op jit(solution)/shard_map/all_gather | solution.py:101
  246.4 2.1 copy-start.1
  317.3 22.7 %copy-start.3 = (f32[384,2]{0,1:T(2,128)S(1)}, f32[384,2]{0,1:T(2,128)}, u32[]{:S(2)}) copy-start(f32[384,2]{0,1:T(2,128)} %param.9) | copy-start | bytes 9220
  317.3 13.3 %all-to-all-start.4 = ((bf16[4,2,1,128,256]{4,3,1,2,0:T(8,128)(2,1)}), bf16[4,2,1,128,256]{4,3,1,2,0:T(8,128)(2,1)S(1)}, u32[]{:S(2)}, u32[]{:S(2)}) async-start(bf16[4,2,1,128,256]{4,3,1,2,0:T(8,128)(2,1)} %copy.26), calls=%async_computation.4 | async-start | bytes 1048576 | tf_op jit(solution)/shard_map/all_to_all | solution.py:49
  330.6 32.8 %all-to-all-start.6 = ((bf16[32,24,256]{2,1,0:T(8,128)(2,1)}), bf16[32,24,256]{2,1,0:T(8,128)(2,1)S(1)}, u32[]{:S(2)}, u32[]{:S(2)}) async-start(bf16[32,24,256]{2,1,0:T(8,128)(2,1)} %bitcast.11), calls=%async_computation.6 | async-start | bytes 786432 | tf_op jit(solution)/shard_map/all_to_all | solution.py:112
Sparse Core Ops, SparseCore 0:
  64.4 65.2 all-gather.2
  250.3 28.7 all-gather.4
